TPU v7x, 32 devices: a whole 2x2x4 slice. The times are simulated.
32 devices in a mesh: ep: 8 (over z, y), tp: 4 (over x, core).
Axes of the slice: x: 2, y: 2, z: 4, core: 2. Of those that a mesh axis runs over, the one named last changes fastest.
Arguments:
- tokens: bfloat16 [2048, 2048], P('ep'), may hold values from -6 to 6
- norm_gain: float32 [2048], replicated, may hold values from 0.1 to 1.9
- expert_ids: int32 [2048, 2], P('ep'), may hold values from 0 to 3, all different within a row; in each aligned block of 256 rows (0 to 255, 256 to 511, ...) at most 160 rows name the same one
- route_weight: float32 [2048, 2], P('ep'), may hold values from 0.2 to 1
- w_gate: bfloat16 [8, 2048, 3584], P('ep', None, 'tp'), may hold values from -0.125 to 0.125
- w_up: bfloat16 [8, 2048, 3584], P('ep', None, 'tp'), may hold values from -0.125 to 0.125
- w_down: bfloat16 [8, 3584, 2048], P('ep', 'tp'), may hold values from -0.0625 to 0.0625
Outputs:
- mixed: bfloat16 [2048, 2048], P('ep', 'tp')
Inputs may be any that keep to these rules, and one draw needn't show every extreme that they name: `expert_ids`: A token names 2 different experts. In each aligned block of 256 tokens (the tokens of one index of ep) no expert is named by more than 160 tokens, a bound that some block reaches.
All inputs are finite; a program needn't handle non-finite values.
Results may differ from a plain program's by a relative error of at most 0.014.
Values may be sent and summed in bfloat16 or wider, within the bound.
A program may use at most 128 MiB of HBM per device.

v0:
```python
import jax
import jax.numpy as jnp
from jax import lax
from jax.sharding import PartitionSpec as P

HALVES = 2


EPSILON = 1e-05


def layer_normed(tokens, norm_gain):
    values = tokens.astype(jnp.float32)
    center = values - jnp.mean(values, axis=-1, keepdims=True)
    spread = jnp.mean(center * center, axis=-1, keepdims=True)
    return (center * lax.rsqrt(spread + EPSILON) * norm_gain).astype(jnp.bfloat16)


def slot_numbers(chosen, experts):
    onehot = (chosen[..., None] == jnp.arange(experts, dtype=jnp.int32)).astype(jnp.int32)
    before = jnp.cumsum(onehot, axis=1) - onehot
    return jnp.sum(before * onehot, axis=-1)


def body(tokens, norm_gain, expert_ids, route_weight, w_gate, w_up, w_down):
    tok_rows, width = tokens.shape
    top_count = expert_ids.shape[1]
    ep_count = lax.axis_size("ep")
    experts = ep_count // HALVES
    capacity = 2 * min(tok_rows // 2, 5 * tok_rows * top_count // (8 * experts))
    normed = layer_normed(tokens, norm_gain)
    padded = jnp.concatenate([normed, jnp.zeros((1, width), jnp.bfloat16)], axis=0)
    slots = slot_numbers(expert_ids.reshape(1, -1), experts).reshape(-1)
    flat_expert = expert_ids.reshape(-1)
    owner = jnp.arange(tok_rows * top_count, dtype=jnp.int32) // top_count
    place = flat_expert * capacity + slots
    table = jnp.full((experts * capacity,), tok_rows, jnp.int32).at[place].set(owner)
    outgoing = padded[table].reshape(experts, capacity, width)
    columns = width // lax.axis_size("tp")
    portion = lax.dynamic_slice_in_dim(outgoing, lax.axis_index("tp") * columns, columns, 2)
    doubled = jnp.repeat(portion, HALVES, axis=0)
    pieces = lax.all_to_all(doubled, "ep", split_axis=0, concat_axis=0, tiled=True)
    arrived = lax.all_gather(pieces, "tp", axis=2, tiled=True)
    routed = arrived.reshape(-1, width)
    gate = jnp.dot(routed, w_gate[0], preferred_element_type=jnp.float32)
    up = jnp.dot(routed, w_up[0], preferred_element_type=jnp.float32)
    hidden = (jax.nn.silu(gate) * up).astype(jnp.bfloat16)
    partial_value = jnp.dot(hidden, w_down[0], preferred_element_type=jnp.float32)
    reduced = lax.psum_scatter(
        partial_value.astype(jnp.bfloat16), "tp", scatter_dimension=1, tiled=True
    )
    returned = lax.all_to_all(
        reduced.reshape(ep_count, capacity, -1), "ep", split_axis=0, concat_axis=0, tiled=True
    )
    quarter = returned.shape[2]
    summed = returned.reshape(experts, HALVES, capacity, quarter).astype(jnp.float32).sum(axis=1)
    picked = summed.reshape(experts * capacity, quarter)[place].reshape(
        tok_rows, top_count, quarter
    )
    mixed = jnp.sum(route_weight[:, :, None] * picked, axis=1)
    return mixed.astype(jnp.bfloat16)


def solution(mesh):
    return jax.shard_map(
        body,
        mesh=mesh,
        in_specs=(
            P("ep", None),
            P(),
            P("ep", None),
            P("ep", None),
            P("ep", None, "tp"),
            P("ep", None, "tp"),
            P("ep", "tp", None),
        ),
        out_specs=P("ep", "tp"),
        check_vma=False,
    )
```

profile of v0, /device:TPU:0, one launch (start us, length us, event | category | flops | bytes accessed | tf_op | source)
XLA Modules:
  0.0 228.1 jit_solution(8858825932461723816)
XLA Ops:
  6.5 0.0 all-gather.2.cloned.1.call-start
  6.5 0.8 copy.11
  7.4 0.1 eq.27
  7.5 1.2 reduce-window.6
  8.8 0.2 slice_reduce_fusion
  9.0 0.7 broadcast_multiply_fusion
  9.7 0.2 reduce-window.9
  9.9 0.1 broadcast.113
  10.0 0.1 copy.10
  10.1 0.1 mul.64
  10.3 2.4 %scatter_custom_fusion = s32[640]{0:T(1024)S(1)} fusion(s32[512]{0:T(512)S(1)} %bitcast.41, s32[512]{0:T(512)S(1)} %add_select_fusion, s32[]{:T(128)} %constant.41.clone.1), kind=kCustom, calls=%fused_computation.35 | custom fusion | bytes 2564 | tf_op jit(solution)/shard_map/scatter | solution.py:37
  12.8 1.4 convert_reduce_fusion
  14.2 1.6 fusion.6
  15.9 1.6 fusion.8
  17.5 0.1 concatenate.3
  17.6 4.1 %gather_fusion = bf16[640,2048]{1,0:T(8,128)(2,1)} fusion(bf16[257,2048]{1,0:T(8,128)(2,1)S(1)} %concatenate.3, s32[1024]{0:T(1024)S(1)} %pad_clamp_fusion.1), kind=kCustom, calls=%fused_computation | custom fusion | bytes 5245440 | tf_op jit(solution)/shard_map/gather | solution.py:38
  21.7 1.1 constant_dynamic-slice_fusion
  22.8 0.1 broadcast_in_dim.8
  22.9 38.6 %all_to_all.10 = bf16[8,160,512]{2,1,0:T(8,128)(2,1)} all-to-all(bf16[8,160,512]{2,1,0:T(8,128)(2,1)S(1)} %bitcast.38), channel_id=1, replica_groups=mesh['ep'=8,'tp'=4] {'ep'}, dimensions={0} | all-to-all | bytes 2621440 | tf_op jit(solution)/shard_map/all_to_all | solution.py:42
  61.5 0.0 all-gather.2.cloned.1.call-update
  61.5 0.0 reduce-scatter.2.cloned.1.call-start
  61.6 39.5 %all-gather.2.cloned.1.call-done = bf16[8,160,2048]{2,1,0:T(8,128)(2,1)} async-done(((bf16[8,160,512]{2,1,0:T(8,128)(2,1)}), bf16[8,160,2048]{2,1,0:T(8,128)(2,1)}) %all-gather.2.cloned.1.call-update) | async-done | bytes 5242896 | tf_op jit(solution)/shard_map/all_gather | solution.py:43
  101.1 10.0 %fusion.2 = f32[1280,896]{1,0:T(8,128)} fusion(bf16[1280,2048]{1,0:T(8,128)(2,1)} %bitcast.45, bf16[1,2048,896]{2,1,0:T(8,128)(2,1)} %param.11), kind=kOutput, calls=%fused_computation.7 | convolution fusion | flops 4697620480 | bytes 13500416 | tf_op jit(solution)/shard_map/dot_general | solution.py:45
  111.1 17.6 %convolution_convert_fusion = bf16[1280,2048]{1,0:T(8,128)(2,1)} fusion(bf16[1,896,2048]{2,1,0:T(8,128)(2,1)} %param.13, f32[1280,896]{1,0:T(8,128)} %fusion.2, bf16[1280,2048]{1,0:T(8,128)(2,1)} %bitcast.46, bf16[1,2048,896]{2,1,0:T(8,128)(2,1)} %param.12), kind=kOutput, calls=%fused_computation.3 | convolution fusion | flops 9404743680 | bytes 22413312 | tf_op jit(solution)/shard_map/dot_general | solution.py:48
  128.6 0.0 copy-start
  128.6 0.0 reduce-scatter.2.cloned.1.call-update
  128.7 51.3 %reduce-scatter.2.cloned.1.call-done = bf16[1280,512]{1,0:T(8,128)(2,1)} async-done(((bf16[1280,2048]{1,0:T(8,128)(2,1)}), bf16[1280,512]{1,0:T(8,128)(2,1)}) %reduce-scatter.2.cloned.1.call-update) | async-done | bytes 1310736 | tf_op jit(solution)/shard_map/reduce_scatter | solution.py:49
  180.0 5.5 %all-to-all-start.1 = ((bf16[8,160,512]{2,1,0:T(8,128)(2,1)}), bf16[8,160,512]{2,1,0:T(8,128)(2,1)S(1)}, u32[]{:S(2)}, u32[]{:S(2)}) async-start(bf16[8,160,512]{2,1,0:T(8,128)(2,1)} %bitcast.40), calls=%async_computation.2 | async-start | bytes 2621440 | tf_op jit(solution)/shard_map/all_to_all | solution.py:52
  185.5 0.0 copy-done
  185.5 0.1 copy.9
  185.7 31.1 %all-to-all-done.1 = bf16[8,160,512]{2,1,0:T(8,128)(2,1)S(1)} async-done(((bf16[8,160,512]{2,1,0:T(8,128)(2,1)}), bf16[8,160,512]{2,1,0:T(8,128)(2,1)S(1)}, u32[]{:S(2)}, u32[]{:S(2)}) %all-to-all-start.1) | async-done | bytes 1310752 | tf_op jit(solution)/shard_map/all_to_all | solution.py:52
  216.7 0.2 convert_reduce_fusion.1
  216.9 1.6 gather_fusion.1
  218.6 0.6 reshape.191
  219.2 2.1 multiply_reduce_fusion
  (13 shorter events, 0.1 us)
Async XLA Ops:
  6.5 94.6 %all-gather.2.cloned.1.call-start = ((), (), s32[]{:S(2)}) async-start(), calls=%async_computation.3 | async-start | bytes 6553600 | tf_op jit(solution)/shard_map/all_gather | solution.py:43
  61.5 118.4 %reduce-scatter.2.cloned.1.call-start = ((), (), s32[]{:S(2)}) async-start(), calls=%async_computation.4 | async-start | bytes 6553600 | tf_op jit(solution)/shard_map/reduce_scatter | solution.py:49
  128.6 56.9 %copy-start = (f32[256,2]{0,1:T(2,128)S(1)}, f32[256,2]{0,1:T(2,128)}, u32[]{:S(2)}) copy-start(f32[256,2]{0,1:T(2,128)} %param.10) | copy-start | bytes 6148
  180.0 36.7 %all-to-all-start.1 = ((bf16[8,160,512]{2,1,0:T(8,128)(2,1)}), bf16[8,160,512]{2,1,0:T(8,128)(2,1)S(1)}, u32[]{:S(2)}, u32[]{:S(2)}) async-start(bf16[8,160,512]{2,1,0:T(8,128)(2,1)} %bitcast.40), calls=%async_computation.2 | async-start | bytes 2621440 | tf_op jit(solution)/shard_map/all_to_all | solution.py:52
Sparse Core Ops, SparseCore 0:
  61.7 39.4 all-gather.1
  128.8 51.1 reduce-scatter.1
where the time goes:
time: 228 us
  waiting for transfers between devices  122 us (54%)
  blocking collectives  38.6 us (17%)
  matrix products  27.5 us (12%)
  between operations  13.6 us (6%)
  local copies, waits for them, and re-layouts  11.8 us (5%)
  other arithmetic  9.14 us (4%)
  starting transfers between devices  5.56 us (2%)
    reduce_scatter x1, waiting for transfers between devices, body(): lax.psum_scatter(partial_value.astype(jnp.bfloat16), 'tp', scatter_dimens...  51.3 us
    all_gather x1, waiting for transfers between devices, body(): arrived = lax.all_gather(pieces, 'tp', axis=2, tiled=True)  39.5 us
    all_to_all x1, blocking collectives, body(): lax.all_to_all(doubled, 'ep', split_axis=0, concat_axis=0, tiled=True)  38.6 us
    all_to_all x1, waiting for transfers between devices, body(): lax.all_to_all(reduced.reshape(ep_count, capacity, -1), 'ep', split_axis=...  31.1 us
    dot_general x1, matrix products, body(): jnp.dot(hidden, w_down[0], preferred_element_type=jnp.float32)  17.6 us
    dot_general x1, matrix products, body(): gate = jnp.dot(routed, w_gate[0], preferred_element_type=jnp.float32)  9.98 us
    all_to_all x1, starting transfers between devices, body(): lax.all_to_all(reduced.reshape(ep_count, capacity, -1), 'ep', split_axis=...  5.52 us
  transfers between devices with their start and end apart: 3, of which 3 were waited for; matrix products, arithmetic and copies ran while one was open for 0% of the time, Pallas kernels for 0%

commit v1 on v0

--- a/solution.py
+++ b/solution.py
@@ -1,12 +1,16 @@
+import functools
+
 import jax
 import jax.numpy as jnp
 from jax import lax
+from jax.experimental import pallas as pl
+from jax.experimental.pallas import tpu as pltpu
 from jax.sharding import PartitionSpec as P
 
 HALVES = 2
-
-
+CORES = 2
 EPSILON = 1e-05
+MESH = pl.DeviceIdType.MESH
 
 
 def layer_normed(tokens, norm_gain):
@@ -22,12 +26,266 @@
     return jnp.sum(before * onehot, axis=-1)
 
 
+def capacity_of(tok_rows, top_count, experts):
+    return 2 * min(tok_rows // 2, 5 * tok_rows * top_count // (8 * experts))
+
+
+def kernel(experts, cap, tokens_ref, gain_ref, ids_ref, weight_ref, wg_hbm, wu_hbm, wd_hbm,
+           out_ref, wg, wu, wd, routed, away, part, mate, chip, hop1, turn, hop2, final, back,
+           load_sem, zs, zr, xs, xr, ys, yr, fs, fr, ds, dr, ms, mr, h1s, h1r, h2s, h2r, bs, br):
+    ep, tp = lax.axis_index("ep"), lax.axis_index("tp")
+    z, y = ep // HALVES, ep % HALVES
+    x, c = tp // CORES, tp % CORES
+    tok_rows, width = tokens_ref.shape
+    quarter = out_ref.shape[1]
+    bf16, f32 = jnp.bfloat16, jnp.float32
+
+    loads = [
+        pltpu.make_async_copy(src.at[0], dst, load_sem.at[i])
+        for i, (src, dst) in enumerate(((wg_hbm, wg), (wu_hbm, wu), (wd_hbm, wd)))
+    ]
+    for load in loads:
+        load.start()
+
+    def device(zz, yy, xx, cc):
+        return (zz * HALVES + yy, xx * CORES + cc)
+
+    x_peer = device(z, y, 1 - x, c)
+    y_peer = device(z, 1 - y, x, c)
+    mate_peer = device(z, y, x, 1 - c)
+    first = (z * HALVES + (c * (1 - y) + (1 - c) * y), (c * x + (1 - c) * (1 - x)) * CORES + c)
+    second = (z * HALVES + (c * y + (1 - c) * (1 - y)), (c * (1 - x) + (1 - c) * x) * CORES + c)
+
+    def z_peer(o):
+        return device((z + o) % experts, y, x, c)
+
+    barrier = pltpu.get_barrier_semaphore()
+    peers = [x_peer, y_peer, mate_peer] + [z_peer(o) for o in range(1, experts)]
+    for peer in peers:
+        pl.semaphore_signal(barrier, inc=1, device_id=peer, device_id_type=MESH)
+
+    ids = ids_ref[...]
+    one, two = ids[:, 0:1], ids[:, 1:2]
+    lane = lax.broadcasted_iota(jnp.int32, (tok_rows, 128), 1)
+    expert = (lane + z) % experts
+    named = jnp.logical_or(one == expert, two == expert)
+    lower = (
+        lax.broadcasted_iota(jnp.int32, (tok_rows, tok_rows), 1)
+        < lax.broadcasted_iota(jnp.int32, (tok_rows, tok_rows), 0)
+    )
+    slot = jnp.dot(
+        lower.astype(f32).astype(bf16), named.astype(f32).astype(bf16), preferred_element_type=f32
+    )
+    slot = jnp.where(named, slot, -1.0).astype(jnp.int32)
+    places = lax.broadcasted_iota(jnp.int32, (tok_rows, cap), 1)
+
+    def chosen(o):
+        return places == slot[:, o:o + 1]
+
+    values = tokens_ref[...].astype(f32)
+    mean = jnp.mean(values, axis=-1, keepdims=True)
+    center = values - mean
+    spread = jnp.mean(center * center, axis=-1, keepdims=True)
+    mine = pl.ds(pl.multiple_of(tp * quarter, quarter), quarter)
+    own = tokens_ref[:, mine].astype(f32) - mean
+    normed = (own * lax.rsqrt(spread + EPSILON) * gain_ref[:, mine]).astype(bf16)
+
+    def outgoing(o):
+        return lax.dot_general(
+            chosen(o).astype(f32).astype(bf16), normed, (((0,), (0,)), ((), ())),
+            preferred_element_type=f32,
+        ).astype(bf16)
+
+    def block(d, yy, xx, cc):
+        rows = pl.ds(pl.multiple_of(yy * cap, cap), cap)
+        columns = pl.ds(pl.multiple_of((xx * CORES + cc) * quarter, quarter), quarter)
+        return routed.at[d, rows, columns]
+
+    def send(src, dst, send_sem, recv_sem, peer):
+        copy = pltpu.make_async_remote_copy(
+            src_ref=src, dst_ref=dst, send_sem=send_sem, recv_sem=recv_sem,
+            device_id=peer, device_id_type=MESH,
+        )
+        copy.start()
+        return copy
+
+    order = sorted(range(experts), key=lambda d: min(d, experts - d))
+    sent = []
+    for o in order:
+        if o:
+            away[o - 1] = outgoing(o)
+    pl.semaphore_wait(barrier, len(peers))
+    z_copies = {}
+    for o in order:
+        if o:
+            d = experts - o
+            z_copies[d] = send(away.at[o - 1], block(d, y, x, c), zs.at[d], zr.at[d], z_peer(o))
+    routed[0, pl.ds(pl.multiple_of(y * cap, cap), cap), mine] = outgoing(0)
+
+    x_copies, y_copies, forwards, pairs, mates = {}, {}, {}, {}, {}
+
+    def launch(d):
+        if d:
+            z_copies[d].wait_recv()
+        b = block(d, y, x, c)
+        x_copies[d] = send(b, b, xs.at[d], xr.at[d], x_peer)
+        y_copies[d] = send(b, b, ys.at[d], yr.at[d], y_peer)
+        pairs[d] = [send(b, b, ds.at[d, 0], dr.at[d, 0], mate_peer)]
+
+    def relay(d):
+        x_copies[d].wait_recv()
+        y_copies[d].wait_recv()
+        b = block(d, c * y + (1 - c) * (1 - y), c * (1 - x) + (1 - c) * x, c)
+        forwards[d] = send(b, b, fs.at[d], fr.at[d], first)
+        for i, b in ((1, block(d, y, 1 - x, c)), (2, block(d, 1 - y, x, c))):
+            pairs[d].append(send(b, b, ds.at[d, i], dr.at[d, i], mate_peer))
+
+    def finish(d):
+        forwards[d].wait_recv()
+        b = block(d, 1 - y, 1 - x, c)
+        pairs[d].append(send(b, b, ds.at[d, 3], dr.at[d, 3], mate_peer))
+        for copy in pairs[d]:
+            copy.wait_recv()
+
+    def columns_of(xx, cc):
+        return pl.ds(pl.multiple_of((xx * CORES + cc) * quarter, quarter), quarter)
+
+    def compute(d):
+        rows = routed[d]
+        gate = jnp.dot(rows, wg[...], preferred_element_type=f32)
+        up = jnp.dot(rows, wu[...], preferred_element_type=f32)
+        hidden = (gate / (1.0 + jnp.exp(-gate)) * up).astype(bf16)
+        if d == 0:
+            loads[2].wait()
+        for xx in range(2):
+            part[d, 1 - c, xx] = jnp.dot(
+                hidden, wd[:, columns_of(xx, 1 - c)], preferred_element_type=f32
+            ).astype(bf16)
+        mates[d] = send(part.at[d, 1 - c], mate.at[d], ms.at[d], mr.at[d], mate_peer)
+        for xx in range(2):
+            part[d, c, xx] = jnp.dot(
+                hidden, wd[:, columns_of(xx, c)], preferred_element_type=f32
+            ).astype(bf16)
+
+    hop1_copies, hop2_copies, back_copies = {}, {}, {}
+
+    def return_first(d):
+        mates[d].wait_recv()
+        for j in (2, 3, 0, 1):
+            low, high = j % 2, j // 2
+            x_low, x_high = (1 - x if low else x), (1 - x if high else x)
+            y_low, y_high = (1 - y if low else y), (1 - y if high else y)
+            xx = c * x_low + (1 - c) * x_high
+            yy = c * y_high + (1 - c) * y_low
+            rows = pl.ds(pl.multiple_of(yy * cap, cap), cap)
+            chip[d, j] = (part[d, c, xx, rows].astype(f32) + mate[d, xx, rows].astype(f32)).astype(bf16)
+            if j == 3:
+                hop1_copies[d] = send(chip.at[d, pl.ds(2, 2)], hop1.at[d], h1s.at[d], h1r.at[d], first)
+
+    def return_second(d):
+        hop1_copies[d].wait_recv()
+        turn[d] = (chip[d, 1].astype(f32) + hop1[d, 1].astype(f32)).astype(bf16)
+        hop2_copies[d] = send(turn.at[d], hop2.at[d], h2s.at[d], h2r.at[d], second)
+
+    def return_third(d):
+        hop2_copies[d].wait_recv()
+        total = chip[d, 0].astype(f32) + hop1[d, 0].astype(f32) + hop2[d].astype(f32)
+        if d == 0:
+            back[0] = total.astype(bf16)
+        else:
+            final[d] = total.astype(bf16)
+            o = experts - d
+            back_copies[d] = send(final.at[d], back.at[o], bs.at[o], br.at[o], z_peer(d))
+
+    launch(order[0])
+    for k, d in enumerate(order):
+        if k + 1 < experts:
+            launch(order[k + 1])
+        relay(d)
+        if k >= 1:
+            return_second(order[k - 1])
+        finish(d)
+        if k == 0:
+            loads[0].wait()
+            loads[1].wait()
+        compute(d)
+        return_first(d)
+        if k >= 1:
+            return_third(order[k - 1])
+    return_second(order[-1])
+    return_third(order[-1])
+
+    total = jnp.zeros((tok_rows, quarter), f32)
+    for o in order:
+        if o:
+            back_copies[experts - o].wait_recv()
+        e = (z + o) % experts
+        share = jnp.where(one == e, weight_ref[:, 0:1], 0.0) + jnp.where(two == e, weight_ref[:, 1:2], 0.0)
+        mix = jnp.where(chosen(o), share, 0.0)
+        high = mix.astype(bf16)
+        low = (mix - high.astype(f32)).astype(bf16)
+        rows = back[o]
+        total += jnp.dot(high, rows, preferred_element_type=f32)
+        total += jnp.dot(low, rows, preferred_element_type=f32)
+    out_ref[...] = total.astype(bf16)
+
+    for group in (z_copies, x_copies, y_copies, forwards, mates, hop1_copies, hop2_copies, back_copies):
+        for d in group:
+            group[d].wait_send()
+    for d in pairs:
+        for copy in pairs[d]:
+            copy.wait_send()
+
+
+def fused_body(tokens, norm_gain, expert_ids, route_weight, w_gate, w_up, w_down):
+    tok_rows, width = tokens.shape
+    experts = lax.axis_size("ep") // HALVES
+    cap = capacity_of(tok_rows, expert_ids.shape[1], experts)
+    tp_count = lax.axis_size("tp")
+    quarter = width // tp_count
+    units = w_gate.shape[2]
+    bf16 = jnp.bfloat16
+    dma = pltpu.SemaphoreType.DMA
+    vmem = pl.BlockSpec(memory_space=pltpu.VMEM)
+    hbm = pl.BlockSpec(memory_space=pl.ANY)
+    one = dma((experts,))
+    return pl.pallas_call(
+        functools.partial(kernel, experts, cap),
+        out_shape=jax.ShapeDtypeStruct((tok_rows, quarter), bf16),
+        in_specs=[vmem, vmem, vmem, vmem, hbm, hbm, hbm],
+        out_specs=vmem,
+        scratch_shapes=[
+            pltpu.VMEM((width, units), bf16),
+            pltpu.VMEM((width, units), bf16),
+            pltpu.VMEM((units, width), bf16),
+            pltpu.VMEM((experts, HALVES * cap, width), bf16),
+            pltpu.VMEM((experts - 1, cap, quarter), bf16),
+            pltpu.VMEM((experts, CORES, 2, HALVES * cap, quarter), bf16),
+            pltpu.VMEM((experts, 2, HALVES * cap, quarter), bf16),
+            pltpu.VMEM((experts, 4, cap, quarter), bf16),
+            pltpu.VMEM((experts, 2, cap, quarter), bf16),
+            pltpu.VMEM((experts, cap, quarter), bf16),
+            pltpu.VMEM((experts, cap, quarter), bf16),
+            pltpu.VMEM((experts, cap, quarter), bf16),
+            pltpu.VMEM((experts, cap, quarter), bf16),
+            dma((3,)),
+            one, one, one, one, one, one, one, one,
+            dma((experts, 4)), dma((experts, 4)),
+            one, one, one, one, one, one, one, one,
+        ],
+        compiler_params=pltpu.CompilerParams(
+            collective_id=0, has_side_effects=True, vmem_limit_bytes=60 * 1024 * 1024
+        ),
+        name="expert_layer",
+    )(tokens, norm_gain.reshape(1, -1), expert_ids, route_weight, w_gate, w_up, w_down)
+
+
 def body(tokens, norm_gain, expert_ids, route_weight, w_gate, w_up, w_down):
     tok_rows, width = tokens.shape
     top_count = expert_ids.shape[1]
     ep_count = lax.axis_size("ep")
     experts = ep_count // HALVES
-    capacity = 2 * min(tok_rows // 2, 5 * tok_rows * top_count // (8 * experts))
+    capacity = capacity_of(tok_rows, top_count, experts)
     normed = layer_normed(tokens, norm_gain)
     padded = jnp.concatenate([normed, jnp.zeros((1, width), jnp.bfloat16)], axis=0)
     slots = slot_numbers(expert_ids.reshape(1, -1), experts).reshape(-1)
@@ -61,9 +319,18 @@
     return mixed.astype(jnp.bfloat16)
 
 
+def choose(*args):
+    tok_rows = args[0].shape[0]
+    experts = lax.axis_size("ep") // HALVES
+    cap = capacity_of(tok_rows, args[2].shape[1], experts)
+    if cap % 16 == 0 and lax.axis_size("tp") == 2 * CORES and args[2].shape[1] == 2:
+        return fused_body(*args)
+    return body(*args)
+
+
 def solution(mesh):
     return jax.shard_map(
-        body,
+        choose,
         mesh=mesh,
         in_specs=(
             P("ep", None),

time: 228 us -> 106 us (0.46)
  waiting for transfers between devices: 122 us -> 0 us
  Pallas kernels: 0 us -> 101 us
  blocking collectives: 38.6 us -> 0 us
  matrix products: 27.5 us -> 0 us
  between operations: 13.6 us -> 0.01 us
  other arithmetic: 9.14 us -> 0 us
  local copies, waits for them, and re-layouts: 11.8 us -> 4.62 us
  starting transfers between devices: 5.56 us -> 0 us
    pallas_call x0 -> x1, Pallas kernels: none -> 101 us  [fused_body(): pl.pallas_call(functools.partial(kernel, experts, cap), out_shape=jax.Sha...]
    reduce_scatter x1 -> x0, waiting for transfers between devices: 51.3 us -> none  [body(): lax.psum_scatter(partial_value.astype(jnp.bfloat16), 'tp', scatter_dimens...]
    all_gather x1 -> x0, waiting for transfers between devices: 39.5 us -> none  [body(): arrived = lax.all_gather(pieces, 'tp', axis=2, tiled=True)]
    all_to_all x1 -> x0, blocking collectives: 38.6 us -> none  [body(): lax.all_to_all(doubled, 'ep', split_axis=0, concat_axis=0, tiled=True)]
    all_to_all x1 -> x0, waiting for transfers between devices: 31.1 us -> none  [body(): lax.all_to_all(reduced.reshape(ep_count, capacity, -1), 'ep', split_axis=...]
    dot_general x2 -> x0, matrix products: 27.5 us -> none  [the longest x1 17.6 us: body(): jnp.dot(hidden, w_down[0], preferred_element_type=jnp.float32)]
    gather x2 -> x0, local copies, waits for them, and re-layouts: 5.71 us -> none  [the longest x1 4.09 us: body(): outgoing = padded[table].reshape(experts, capacity, width)]
    all_to_all x1 -> x0, starting transfers between devices: 5.52 us -> none  [body(): lax.all_to_all(reduced.reshape(ep_count, capacity, -1), 'ep', split_axis=...]
  transfers between devices with their start and end apart: 3 -> 0, of which waited for: 3 -> 0; matrix products, arithmetic and copies ran while one was open for 0% -> 0% of each run, Pallas kernels for 0% -> 0%
where the time goes in v1:
time: 106 us
  Pallas kernels  101 us (95%)
  local copies, waits for them, and re-layouts  4.62 us (4%)
    pallas_call x1, Pallas kernels, fused_body(): pl.pallas_call(functools.partial(kernel, experts, cap), out_shape=jax.Sha...  101 us
    unnamed x3, local copies, waits for them, and re-layouts  4.62 us

profile of v1, /device:TPU:0, one launch (start us, length us, event | category | flops | bytes accessed | tf_op | source)
XLA Modules:
  0.0 105.9 jit_solution(815674291840933968)
XLA Ops:
  0.0 1.5 %copy.8.ids_ref = s32[256,2]{1,0:T(8,128)} copy(s32[256,2]{0,1:T(2,128)} %param.9) | data formatting | bytes 4096 | tf_op args[2]
  1.5 1.5 %copy.9.weight_ref = f32[256,2]{1,0:T(8,128)} copy(f32[256,2]{0,1:T(2,128)} %param.10) | data formatting | bytes 4096 | tf_op args[3]
  3.0 101.3 %expert_layer.1 = bf16[256,512]{1,0:T(8,128)(2,1)} custom-call(bf16[256,2048]{1,0:T(8,128)(2,1)} %tokens_ref.1, f32[1,2048]{1,0:T(1,128)} %bitcast.1, s32[256,2]{1,0:T(8,128)} %copy.8.ids_ref, f32[256,2]{1,0:T(8,128)} %copy.9.weight_ref, bf16[1,2048,896]{2,1,0:T(8,128)(2,1)} %wg_hbm.1, bf16[1,2048,896]{2,1,0:T(8,128)(2,1)} %wu_hbm.1, ...), custom_call_target="tpu_custom_call" | custom-call | tf_op jit(solution)/shard_map/expert_layer/pallas_call | solution.py:252
  104.3 1.7 %copy.11 = bf16[256,512]{1,0:T(8,128)(2,1)} copy(bf16[256,512]{1,0:T(8,128)(2,1)} %expert_layer.1) | data formatting | bytes 524288

commit v2 on v1

--- a/solution.py
+++ b/solution.py
@@ -31,7 +31,7 @@
 
 
 def kernel(experts, cap, tokens_ref, gain_ref, ids_ref, weight_ref, wg_hbm, wu_hbm, wd_hbm,
-           out_ref, wg, wu, wd, routed, away, part, mate, chip, hop1, turn, hop2, final, back,
+           out_hbm, wg, wu, wd, out_ref, routed, away, part, mate, chip, hop1, turn, hop2, final, back,
            load_sem, zs, zr, xs, xr, ys, yr, fs, fr, ds, dr, ms, mr, h1s, h1r, h2s, h2r, bs, br):
     ep, tp = lax.axis_index("ep"), lax.axis_index("tp")
     z, y = ep // HALVES, ep % HALVES
@@ -64,7 +64,7 @@
     for peer in peers:
         pl.semaphore_signal(barrier, inc=1, device_id=peer, device_id_type=MESH)
 
-    ids = ids_ref[...]
+    ids = jnp.transpose(ids_ref[...])
     one, two = ids[:, 0:1], ids[:, 1:2]
     lane = lax.broadcasted_iota(jnp.int32, (tok_rows, 128), 1)
     expert = (lane + z) % experts
@@ -109,8 +109,8 @@
         copy.start()
         return copy
 
-    order = sorted(range(experts), key=lambda d: min(d, experts - d))
-    sent = []
+    order = [0] + sorted(range(1, experts), key=lambda d: -min(d, experts - d))
+    turns = order
     for o in order:
         if o:
             away[o - 1] = outgoing(o)
@@ -150,12 +150,13 @@
     def columns_of(xx, cc):
         return pl.ds(pl.multiple_of((xx * CORES + cc) * quarter, quarter), quarter)
 
-    def compute(d):
+    def compute(d, early, between):
         rows = routed[d]
         gate = jnp.dot(rows, wg[...], preferred_element_type=f32)
         up = jnp.dot(rows, wu[...], preferred_element_type=f32)
         hidden = (gate / (1.0 + jnp.exp(-gate)) * up).astype(bf16)
-        if d == 0:
+        between()
+        if early:
             loads[2].wait()
         for xx in range(2):
             part[d, 1 - c, xx] = jnp.dot(
@@ -197,30 +198,44 @@
             o = experts - d
             back_copies[d] = send(final.at[d], back.at[o], bs.at[o], br.at[o], z_peer(d))
 
-    launch(order[0])
-    for k, d in enumerate(order):
-        if k + 1 < experts:
-            launch(order[k + 1])
-        relay(d)
-        if k >= 1:
-            return_second(order[k - 1])
+    look = 2
+    for k in range(look):
+        launch(order[k])
+    for k in range(look - 1):
+        relay(order[k])
+
+    def ahead(k):
+        if k + look < experts:
+            launch(order[k + look])
+        if k + look - 1 < experts:
+            relay(order[k + look - 1])
+
+    for k, d in enumerate(turns):
+        def between(k=k):
+            pass
+            if k >= 1:
+                return_second(turns[k - 1])
+
+        ahead(k)
         finish(d)
         if k == 0:
             loads[0].wait()
             loads[1].wait()
-        compute(d)
+        compute(d, k == 0, between)
         return_first(d)
-        if k >= 1:
-            return_third(order[k - 1])
-    return_second(order[-1])
-    return_third(order[-1])
+        if k >= 2:
+            return_third(turns[k - 2])
+    return_second(turns[-1])
+    return_third(turns[-2])
+    return_third(turns[-1])
 
     total = jnp.zeros((tok_rows, quarter), f32)
+    route = jnp.transpose(weight_ref[...])
     for o in order:
         if o:
             back_copies[experts - o].wait_recv()
         e = (z + o) % experts
-        share = jnp.where(one == e, weight_ref[:, 0:1], 0.0) + jnp.where(two == e, weight_ref[:, 1:2], 0.0)
+        share = jnp.where(one == e, route[:, 0:1], 0.0) + jnp.where(two == e, route[:, 1:2], 0.0)
         mix = jnp.where(chosen(o), share, 0.0)
         high = mix.astype(bf16)
         low = (mix - high.astype(f32)).astype(bf16)
@@ -228,6 +243,8 @@
         total += jnp.dot(high, rows, preferred_element_type=f32)
         total += jnp.dot(low, rows, preferred_element_type=f32)
     out_ref[...] = total.astype(bf16)
+    store = pltpu.make_async_copy(out_ref, out_hbm, load_sem.at[3])
+    store.start()
 
     for group in (z_copies, x_copies, y_copies, forwards, mates, hop1_copies, hop2_copies, back_copies):
         for d in group:
@@ -235,6 +252,7 @@
     for d in pairs:
         for copy in pairs[d]:
             copy.wait_send()
+    store.wait()
 
 
 def fused_body(tokens, norm_gain, expert_ids, route_weight, w_gate, w_up, w_down):
@@ -253,11 +271,12 @@
         functools.partial(kernel, experts, cap),
         out_shape=jax.ShapeDtypeStruct((tok_rows, quarter), bf16),
         in_specs=[vmem, vmem, vmem, vmem, hbm, hbm, hbm],
-        out_specs=vmem,
+        out_specs=hbm,
         scratch_shapes=[
             pltpu.VMEM((width, units), bf16),
             pltpu.VMEM((width, units), bf16),
             pltpu.VMEM((units, width), bf16),
+            pltpu.VMEM((tok_rows, quarter), bf16),
             pltpu.VMEM((experts, HALVES * cap, width), bf16),
             pltpu.VMEM((experts - 1, cap, quarter), bf16),
             pltpu.VMEM((experts, CORES, 2, HALVES * cap, quarter), bf16),
@@ -268,7 +287,7 @@
             pltpu.VMEM((experts, cap, quarter), bf16),
             pltpu.VMEM((experts, cap, quarter), bf16),
             pltpu.VMEM((experts, cap, quarter), bf16),
-            dma((3,)),
+            dma((4,)),
             one, one, one, one, one, one, one, one,
             dma((experts, 4)), dma((experts, 4)),
             one, one, one, one, one, one, one, one,
@@ -277,7 +296,7 @@
             collective_id=0, has_side_effects=True, vmem_limit_bytes=60 * 1024 * 1024
         ),
         name="expert_layer",
-    )(tokens, norm_gain.reshape(1, -1), expert_ids, route_weight, w_gate, w_up, w_down)
+    )(tokens, norm_gain.reshape(1, -1), expert_ids.T, route_weight.T, w_gate, w_up, w_down)
 
 
 def body(tokens, norm_gain, expert_ids, route_weight, w_gate, w_up, w_down):

time: 106 us -> 79.8 us (0.75)
  Pallas kernels: 101 us -> 77.9 us
  local copies, waits for them, and re-layouts: 4.62 us -> 1.67 us
    pallas_call x1, Pallas kernels: 101 us -> 77.9 us  [fused_body(): pl.pallas_call(functools.partial(kernel, experts, cap), out_shape=jax.Sha...]
    unnamed x3 -> x1, local copies, waits for them, and re-layouts: 4.62 us -> 1.67 us
where the time goes in v2:
time: 79.8 us; the launch traced here: 79.6 us
  Pallas kernels  77.9 us (98%)
  local copies, waits for them, and re-layouts  1.67 us (2%)
    pallas_call x1, Pallas kernels, fused_body(): pl.pallas_call(functools.partial(kernel, experts, cap), out_shape=jax.Sha...  77.9 us
    unnamed x1, local copies, waits for them, and re-layouts  1.67 us

profile of v2, /device:TPU:0, one launch (start us, length us, event | category | flops | bytes accessed | tf_op | source)
XLA Modules:
  0.0 79.6 jit_solution(5490597525705432121)
XLA Ops:
  0.0 77.9 %expert_layer.1 = bf16[256,512]{1,0:T(8,128)(2,1)} custom-call(bf16[256,2048]{1,0:T(8,128)(2,1)} %tokens_ref.1, f32[1,2048]{1,0:T(1,128)} %bitcast.3, s32[2,256]{1,0:T(2,128)} %bitcast.4, f32[2,256]{1,0:T(2,128)} %bitcast.5, bf16[1,2048,896]{2,1,0:T(8,128)(2,1)} %wg_hbm.1, bf16[1,2048,896]{2,1,0:T(8,128)(2,1)} %wu_hbm.1, bf16[1,896,2048]{2,1,0:T(8,128)(2,1)} %wd_hbm.1), custom_call_target="tpu_custom_call" | custom-call | tf_op jit(solution)/shard_map/expert_layer/pallas_call | solution.py:270
  77.9 1.7 %copy.9 = bf16[256,512]{1,0:T(8,128)(2,1)} copy(bf16[256,512]{1,0:T(8,128)(2,1)} %expert_layer.1) | data formatting | bytes 524288
